TPU v7x, 32 devices: a whole 2x2x4 slice. The times are simulated.
32 devices in a mesh: ep: 8 (over z, core), tp: 4 (over y, x).
Axes of the slice: x: 2, y: 2, z: 4, core: 2. Of those that a mesh axis runs over, the one named last changes fastest.
Arguments:
- attn_in: bfloat16 [4096, 2048], P('ep'), may hold values from -6 to 6
- mix_gain: float32 [2048], replicated, may hold values from 0.1 to 1.9
- query_weight: bfloat16 [2048, 1024], P(None, 'tp'), may hold values from -0.125 to 0.125
- key_weight: bfloat16 [2048, 1024], P(None, 'tp'), may hold values from -0.125 to 0.125
- value_weight: bfloat16 [2048, 1024], P(None, 'tp'), may hold values from -0.125 to 0.125
- query_gain: float32 [64], replicated, may hold values from 0.7 to 6
- key_gain: float32 [64], replicated, may hold values from 0.7 to 6
- log_cache: float32 [4096, 16], P('ep', 'tp'), as said below
- head_gain: float32 [1024], P('tp'), may hold values from 0.1 to 1.9
- out_weight: bfloat16 [1024, 2048], P(None, 'tp'), may hold values from -0.1875 to 0.1875
- moe_in: bfloat16 [1024, 2048], P('ep'), may hold values from -6 to 6
- moe_gain: float32 [2048], replicated, may hold values from 0.1 to 1.9
- routes: int32 [1024, 2], P('ep'), may hold values from 0 to 7, all different within a row; in each aligned block of 128 rows (0 to 127, 128 to 255, ...) at most 48 rows name the same one
- route_weight: float32 [1024, 2], P('ep'), may hold values from 0.25 to 1
- expert_gate: bfloat16 [8, 2048, 1024], P('ep', None, 'tp'), may hold values from -0.125 to 0.125
- expert_up: bfloat16 [8, 2048, 1024], P('ep', None, 'tp'), may hold values from -0.125 to 0.125
- expert_down: bfloat16 [8, 1024, 2048], P('ep', 'tp'), may hold values from -0.1875 to 0.1875
Outputs:
- mixer_out: bfloat16 [4096, 2048], P('ep', 'tp')
- moe_out: bfloat16 [1024, 2048], P('ep', 'tp')
Inputs may be any that keep to these rules, and one draw needn't show every extreme that they name: `routes`: each row names 2 different experts; within the rows of one index of ep (aligned blocks of 128 rows) no expert is named by more than 48 rows. `log_cache`: never increasing along positions for each head.
All inputs are finite; a program needn't handle non-finite values.
Results may differ from a plain program's by a relative error of at most 0.015.
The roundings to bfloat16 on the way count: a program that leaves them out, or rounds other values in their place, can miss the bound.
Values may be sent and summed in bfloat16 or wider, within the bound.
A program may use at most 64 MiB of HBM per device.

v0:
```python
import math
import jax
import jax.numpy as jnp
from jax import lax
from jax.sharding import PartitionSpec as P

HD = 64
epsilon = 1e-06


def row_norm(inputs, gain_vec):
    floats = inputs.astype(jnp.float32)
    scaled = floats * lax.rsqrt(jnp.mean(floats * floats, axis=-1, keepdims=True) + epsilon)
    return scaled * gain_vec


def body(
    attn_in,
    mix_gain,
    query_weight,
    key_weight,
    value_weight,
    query_gain,
    key_gain,
    log_cache,
    head_gain,
    out_weight,
    moe_in,
    moe_gain,
    routes,
    route_weight,
    expert_gate,
    expert_up,
    expert_down,
):
    tok_rows = attn_in.shape[0]
    local_heads = query_weight.shape[1] // HD
    normed = row_norm(attn_in, mix_gain).astype(jnp.bfloat16)

    def project(weight):
        return jnp.dot(normed, weight, preferred_element_type=jnp.float32).reshape(
            tok_rows, local_heads, HD
        )

    queries = row_norm(project(query_weight), query_gain).astype(jnp.bfloat16)
    key_rows = (
        row_norm(project(key_weight), key_gain)
        .astype(jnp.bfloat16)
        .reshape(tok_rows, local_heads * HD)
    )
    value_rows = project(value_weight).astype(jnp.bfloat16).reshape(tok_rows, local_heads * HD)
    all_gates = lax.all_gather(log_cache, "ep", axis=0, tiled=True)
    query_pos = lax.axis_index("ep") * tok_rows + jnp.arange(tok_rows, dtype=jnp.int32)
    query_gates = jnp.transpose(log_cache)[:, :, None]
    score_scale = HD ** (-0.5)
    init_state = (
        jnp.full((local_heads, tok_rows), -1e30, jnp.float32),
        jnp.zeros((local_heads, tok_rows), jnp.float32),
        jnp.zeros((local_heads, tok_rows, HD), jnp.float32),
    )
    key_piece = lax.all_gather(key_rows, "ep", axis=0, tiled=True)
    value_piece = lax.all_gather(value_rows, "ep", axis=0, tiled=True)
    span_len = key_piece.shape[0]
    block_len = math.gcd(span_len, 512)

    def block_step(block_index, running):
        running_max, running_sum, weighted = running
        block_begin = block_index * block_len
        key_block = lax.dynamic_slice_in_dim(key_piece, block_begin, block_len, 0).reshape(
            block_len, local_heads, HD
        )
        value_block = lax.dynamic_slice_in_dim(value_piece, block_begin, block_len, 0).reshape(
            block_len, local_heads, HD
        )
        gate_block = lax.dynamic_slice_in_dim(all_gates, block_begin, block_len, 0)
        scores = (
            jnp.einsum("qhd,khd->hqk", queries, key_block, preferred_element_type=jnp.float32)
            * score_scale
        )
        scores = scores + query_gates - jnp.transpose(gate_block)[:, None, :]
        key_pos = block_begin + jnp.arange(block_len, dtype=jnp.int32)
        causal = (key_pos[None, :] <= query_pos[:, None])[None]
        new_max = jnp.maximum(running_max, jnp.max(jnp.where(causal, scores, -1e30), axis=2))
        expo_scores = jnp.where(causal, jnp.exp(scores - new_max[:, :, None]), 0.0)
        rescale = jnp.exp(running_max - new_max)
        running_sum = running_sum * rescale + jnp.sum(expo_scores, axis=2)
        weighted = weighted * rescale[:, :, None] + jnp.einsum(
            "hqk,khd->hqd",
            expo_scores.astype(jnp.bfloat16),
            value_block,
            preferred_element_type=jnp.float32,
        )
        return (new_max, running_sum, weighted)

    final_max, final_sum, weighted = lax.fori_loop(0, span_len // block_len, block_step, init_state)
    attended = jnp.transpose(weighted / final_sum[:, :, None], (1, 0, 2))
    head_out = (
        row_norm(attended, head_gain.reshape(local_heads, HD))
        .astype(jnp.bfloat16)
        .reshape(tok_rows, local_heads * HD)
    )
    mixer_out = jnp.dot(
        lax.all_gather(head_out, "tp", axis=1, tiled=True),
        out_weight,
        preferred_element_type=jnp.float32,
    ).astype(jnp.bfloat16)
    moe_rows = moe_in.shape[0]
    top_count = routes.shape[1]
    local_experts = expert_gate.shape[0]
    senders = lax.axis_size("ep")
    expert_count = local_experts * senders
    capacity = 3 * moe_rows * top_count // (2 * expert_count)
    model_width = moe_in.shape[1]
    moe_normed = row_norm(moe_in, moe_gain).astype(jnp.bfloat16)
    flat_routes = routes.reshape(-1)
    one_hot = (flat_routes[:, None] == jnp.arange(expert_count, dtype=jnp.int32)[None, :]).astype(
        jnp.int32
    )
    order_in = jnp.sum(jnp.cumsum(one_hot, axis=0) * one_hot, axis=1) - 1
    slot_index = flat_routes * capacity + order_in
    token_of = jnp.arange(flat_routes.shape[0], dtype=jnp.int32) // top_count
    source_row = jnp.zeros((expert_count * capacity,), jnp.int32).at[slot_index].set(token_of)
    filled = jnp.zeros((expert_count * capacity,), jnp.bool_).at[slot_index].set(True)
    send_buffer = jnp.where(
        filled[:, None], moe_normed[source_row], jnp.zeros((), jnp.bfloat16)
    ).reshape(expert_count, capacity, model_width)
    share_width = model_width // lax.axis_size("tp")
    share_part = lax.dynamic_slice_in_dim(
        send_buffer, lax.axis_index("tp") * share_width, share_width, 2
    )
    arrived = lax.all_to_all(share_part, "ep", split_axis=0, concat_axis=0, tiled=True)
    piece_now = lax.all_gather(arrived, "tp", axis=2, tiled=True)
    piece_cols = piece_now.shape[2]
    piece_rows = piece_now.reshape(senders, local_experts, capacity, piece_cols)
    gate_next = jnp.einsum(
        "sjcd,jdf->sjcf", piece_rows, expert_gate, preferred_element_type=jnp.float32
    )
    up_next = jnp.einsum(
        "sjcd,jdf->sjcf", piece_rows, expert_up, preferred_element_type=jnp.float32
    )
    hidden = (jax.nn.silu(gate_next) * up_next).astype(jnp.bfloat16)
    partial_value = jnp.einsum(
        "sjcf,jfd->sjcd", hidden, expert_down, preferred_element_type=jnp.float32
    )
    summed = lax.psum_scatter(
        partial_value.astype(jnp.bfloat16), "tp", scatter_dimension=3, tiled=True
    )
    out_cols = summed.shape[3]
    returned = lax.all_to_all(
        summed.reshape(expert_count, capacity, out_cols),
        "ep",
        split_axis=0,
        concat_axis=0,
        tiled=True,
    )
    picked = returned.reshape(expert_count * capacity, out_cols)[slot_index].astype(jnp.float32)
    weighted_rows = picked * route_weight.reshape(-1)[:, None]
    moe_out = jnp.sum(weighted_rows.reshape(moe_rows, top_count, out_cols), axis=1).astype(
        jnp.bfloat16
    )
    return (mixer_out, moe_out)


def solution(mesh):
    in_specs = (
        P("ep", None),
        P(),
        P(None, "tp"),
        P(None, "tp"),
        P(None, "tp"),
        P(),
        P(),
        P("ep", "tp"),
        P("tp"),
        P(None, "tp"),
        P("ep", None),
        P(),
        P("ep", None),
        P("ep", None),
        P("ep", None, "tp"),
        P("ep", None, "tp"),
        P("ep", "tp", None),
    )
    out_specs = (P("ep", "tp"), P("ep", "tp"))
    return jax.shard_map(body, mesh=mesh, in_specs=in_specs, out_specs=out_specs, check_vma=False)
```

profile of v0, /device:TPU:0, one launch (start us, length us, event | category | flops | bytes accessed | tf_op | source)
XLA Modules:
  0.0 263.2 jit_solution(7645723227461239029)
XLA Ops:
  7.2 0.9 copy.25
  10.3 1.4 scatter_custom_fusion.1
  11.7 1.2 fusion.23
  13.0 1.5 scatter_custom_fusion
  14.5 1.2 fusion.25
  15.8 2.5 gather_fusion
  18.4 18.8 %all_to_all.10 = bf16[8,48,512]{2,1,0:T(8,128)(2,1)} all-to-all(bf16[8,48,512]{2,1,0:T(8,128)(2,1)S(1)} %dynamic-slice_select_fusion), channel_id=1, replica_groups=mesh['ep'=8,'tp'=4] {'ep'}, dimensions={0} | all-to-all | bytes 786432 | tf_op jit(solution)/shard_map/all_to_all | solution.py:131
  37.4 2.2 fusion.16
  39.6 2.8 %bitcast_reduce_fusion = (f32[512,4]{0,1:T(4,128)S(1)}, f32[512,256]{0,1:T(8,128)S(1)}) fusion(bf16[2048,256]{1,0:T(8,128)(2,1)} %param.22, bf16[512,2048]{1,0:T(8,128)(2,1)} %param.19, f32[2048]{0:T(1024)S(1)} %copy-done.8, f32[512]{0:T(512)S(1)} %add_rsqrt_fusion.3), kind=kOutput, calls=%fused_computation.59 | convolution fusion | flops 541325312 | bytes 3688448 | tf_op jit(solution)/shard_map/dot_general | solution.py:41
  43.4 2.7 %convolution_convert_fusion.2 = bf16[512,256]{1,0:T(8,128)(2,1)} fusion(bf16[2048,256]{1,0:T(8,128)(2,1)} %param.23, bf16[512,2048]{1,0:T(8,128)(2,1)S(1)} %copy-done.1, f32[2048]{0:T(1024)S(1)} %copy-done.8, f32[512]{0:T(512)S(1)} %add_rsqrt_fusion.3), kind=kOutput, calls=%fused_computation.42 | convolution fusion | flops 541196288 | bytes 3418112 | tf_op jit(solution)/shard_map/dot_general | solution.py:41
  46.3 14.0 %all_gather.16 = f32[4096,4]{0,1:T(4,128)S(1)} all-gather(f32[512,4]{0,1:T(4,128)S(1)} %copy-done.3), channel_id=1, replica_groups=mesh['ep'=8,'tp'=4] {'ep'}, dimensions={0}, use_global_device_ids=true | all-gather | bytes 73728 | tf_op jit(solution)/shard_map/all_gather | solution.py:52
  60.2 2.2 multiply_reduce_fusion.1
  62.5 4.5 %all-gather.11.cloned.1.call-done = bf16[8,48,2048]{2,1,0:T(8,128)(2,1)} async-done(((bf16[8,48,512]{2,1,0:T(8,128)(2,1)}), bf16[8,48,2048]{2,1,0:T(8,128)(2,1)}) %all-gather.11.cloned.1.call-update) | async-done | bytes 1572880 | tf_op jit(solution)/shard_map/all_gather | solution.py:132
  67.0 2.3 convolution_bitcast_fusion.1
  69.3 4.8 %fusion.19 = bf16[8,1,48,2048]{3,2,0,1:T(8,128)(2,1)} fusion(bf16[1,256,2048]{2,1,0:T(8,128)(2,1)S(1)} %copy-done, bf16[8,48,2048]{2,1,0:T(8,128)(2,1)} %all-gather.11.cloned.1.call-done, bf16[1,2048,256]{2,1,0:T(8,128)(2,1)} %param.34, f32[8,1,48,256]{3,2,0,1:T(8,128)S(1)} %convolution_bitcast_fusion.1), kind=kOutput, calls=%fused_computation.35 | convolution fusion | flops 806682624 | bytes 5636096 | tf_op jit(solution)/shard_map/sjcf,jfd->sjcd/dot_general | solution.py:142
  74.4 23.4 %all-gather.5.cloned.1.call-done = bf16[4096,256]{0,1:T(8,128)(2,1)} async-done(((bf16[512,256]{0,1:T(8,128)(2,1)}), bf16[4096,256]{0,1:T(8,128)(2,1)}) %all-gather.5.cloned.1.call-update) | async-done | bytes 2097168 | tf_op jit(solution)/shard_map/all_gather | solution.py:61
  97.8 30.2 %all-gather.7.cloned.1.call-done = bf16[4096,256]{1,0:T(8,128)(2,1)} async-done(((bf16[512,256]{1,0:T(8,128)(2,1)}), bf16[4096,256]{1,0:T(8,128)(2,1)}) %all-gather.7.cloned.1.call-update) | async-done | bytes 2097168 | tf_op jit(solution)/shard_map/all_gather | solution.py:62
  128.0 95.6 %while.18 = (s32[]{:T(128)}, f32[4,512]{1,0:T(4,128)S(1)}, f32[4,512]{1,0:T(4,128)S(1)}, f32[4,512,64]{1,2,0:T(8,128)S(1)}, bf16[4096,256]{0,1:T(8,128)(2,1)}, /...) while((s32[]{:T(128)}, f32[4,512]{1,0:T(4,128)S(1)}, ...), condition=%wide.region_6.7_spmd.clone, body=%wide.region_3.6_spmd.clone.sunk | while | flops 286927872 | bytes 17244372 | solution.py:95
  128.0 1.0 constant_dynamic-slice_fusion.4
  129.2 3.1 %fusion.76 = (f32[4,512]{1,0:T(4,128)S(1)}, f32[4,512,512]{2,1,0:T(8,128)}) fusion(f32[4,512]{1,0:T(4,128)S(1)} %dynamic-slice_bitcast_fusion.2, f32[4,512]{1,0:T(4,128)S(1)} %bitcast.137, pred[512,512]{0,1:T(8,128)(4,1)S(1)} %broadcast_compare_fusion.2, bf16[512,4,64]{0,2,1:T(8,128)(2,1)S(1)} %bitcast.131, ...), kind=kOutput, calls=%fused_computation.7.clone.1 | convolution fusion | flops 139458560 | bytes 5005312 | tf_op jit(solution)/shard_map/while/body/eval_jaxpr/qhd,khd->hqk/dot_general | solution.py:77
  132.3 2.9 %fusion.77 = f32[4,512]{1,0:T(4,128)S(1)} fusion(f32[4,512,512]{2,1,0:T(8,128)} %get-tuple-element.330, f32[4,512]{1,0:T(4,128)S(1)} %select_maximum_fusion.2, f32[4,512]{1,0:T(4,128)S(1)} %dynamic-slice_bitcast_fusion.2, f32[4,512]{1,0:T(4,128)S(1)} %bitcast.138, pred[512,512]{0,1:T(8,128)(4,1)S(1)} %broadcast_compare_fusion.2), kind=kLoop, calls=%fused_computation.12.clone.1 | loop fusion | flops 6289408 | bytes 4489216 | tf_op jit(solution)/shard_map/while/body/eval_jaxpr/reduce_sum | solution.py:86
  135.3 1.0 constant_dynamic-slice_fusion.5
  136.4 3.5 %fusion.79 = f32[4,512,64]{1,2,0:T(8,128)S(1)} fusion(bf16[512,4,64]{0,2,1:T(8,128)(2,1)S(1)} %bitcast.132, f32[4,512,512]{2,1,0:T(8,128)} %get-tuple-element.330, f32[4,512]{1,0:T(4,128)S(1)} %select_maximum_fusion.2, f32[4,512]{1,0:T(4,128)S(1)} %dynamic-slice_bitcast_fusion.2, f32[4,512]{1,0:T(4,128)S(1)} %bitcast.139, ...), kind=kOutput, calls=%fused_computation.15.clone.1 | convolution fusion | flops 140902400 | bytes 5799937 | tf_op jit(solution)/shard_map/while/body/eval_jaxpr/hqk,khd->hqd/dot_general | solution.py:87
  140.0 1.0 constant_dynamic-slice_fusion.4
  141.2 3.1 %fusion.76 = (f32[4,512]{1,0:T(4,128)S(1)}, f32[4,512,512]{2,1,0:T(8,128)}) fusion(f32[4,512]{1,0:T(4,128)S(1)} %dynamic-slice_bitcast_fusion.2, f32[4,512]{1,0:T(4,128)S(1)} %bitcast.137, pred[512,512]{0,1:T(8,128)(4,1)S(1)} %broadcast_compare_fusion.2, bf16[512,4,64]{0,2,1:T(8,128)(2,1)S(1)} %bitcast.131, ...), kind=kOutput, calls=%fused_computation.7.clone.1 | convolution fusion | flops 139458560 | bytes 5005312 | tf_op jit(solution)/shard_map/while/body/eval_jaxpr/qhd,khd->hqk/dot_general | solution.py:77
  144.3 3.0 %fusion.77 = f32[4,512]{1,0:T(4,128)S(1)} fusion(f32[4,512,512]{2,1,0:T(8,128)} %get-tuple-element.330, f32[4,512]{1,0:T(4,128)S(1)} %select_maximum_fusion.2, f32[4,512]{1,0:T(4,128)S(1)} %dynamic-slice_bitcast_fusion.2, f32[4,512]{1,0:T(4,128)S(1)} %bitcast.138, pred[512,512]{0,1:T(8,128)(4,1)S(1)} %broadcast_compare_fusion.2), kind=kLoop, calls=%fused_computation.12.clone.1 | loop fusion | flops 6289408 | bytes 4489216 | tf_op jit(solution)/shard_map/while/body/eval_jaxpr/reduce_sum | solution.py:86
  147.3 1.0 constant_dynamic-slice_fusion.5
  148.4 3.5 %fusion.79 = f32[4,512,64]{1,2,0:T(8,128)S(1)} fusion(bf16[512,4,64]{0,2,1:T(8,128)(2,1)S(1)} %bitcast.132, f32[4,512,512]{2,1,0:T(8,128)} %get-tuple-element.330, f32[4,512]{1,0:T(4,128)S(1)} %select_maximum_fusion.2, f32[4,512]{1,0:T(4,128)S(1)} %dynamic-slice_bitcast_fusion.2, f32[4,512]{1,0:T(4,128)S(1)} %bitcast.139, ...), kind=kOutput, calls=%fused_computation.15.clone.1 | convolution fusion | flops 140902400 | bytes 5799937 | tf_op jit(solution)/shard_map/while/body/eval_jaxpr/hqk,khd->hqd/dot_general | solution.py:87
  152.0 1.0 constant_dynamic-slice_fusion.4
  153.2 3.1 %fusion.76 = (f32[4,512]{1,0:T(4,128)S(1)}, f32[4,512,512]{2,1,0:T(8,128)}) fusion(f32[4,512]{1,0:T(4,128)S(1)} %dynamic-slice_bitcast_fusion.2, f32[4,512]{1,0:T(4,128)S(1)} %bitcast.137, pred[512,512]{0,1:T(8,128)(4,1)S(1)} %broadcast_compare_fusion.2, bf16[512,4,64]{0,2,1:T(8,128)(2,1)S(1)} %bitcast.131, ...), kind=kOutput, calls=%fused_computation.7.clone.1 | convolution fusion | flops 139458560 | bytes 5005312 | tf_op jit(solution)/shard_map/while/body/eval_jaxpr/qhd,khd->hqk/dot_general | solution.py:77
  156.3 2.9 %fusion.77 = f32[4,512]{1,0:T(4,128)S(1)} fusion(f32[4,512,512]{2,1,0:T(8,128)} %get-tuple-element.330, f32[4,512]{1,0:T(4,128)S(1)} %select_maximum_fusion.2, f32[4,512]{1,0:T(4,128)S(1)} %dynamic-slice_bitcast_fusion.2, f32[4,512]{1,0:T(4,128)S(1)} %bitcast.138, pred[512,512]{0,1:T(8,128)(4,1)S(1)} %broadcast_compare_fusion.2), kind=kLoop, calls=%fused_computation.12.clone.1 | loop fusion | flops 6289408 | bytes 4489216 | tf_op jit(solution)/shard_map/while/body/eval_jaxpr/reduce_sum | solution.py:86
  159.2 1.0 constant_dynamic-slice_fusion.5
  160.4 3.6 %fusion.79 = f32[4,512,64]{1,2,0:T(8,128)S(1)} fusion(bf16[512,4,64]{0,2,1:T(8,128)(2,1)S(1)} %bitcast.132, f32[4,512,512]{2,1,0:T(8,128)} %get-tuple-element.330, f32[4,512]{1,0:T(4,128)S(1)} %select_maximum_fusion.2, f32[4,512]{1,0:T(4,128)S(1)} %dynamic-slice_bitcast_fusion.2, f32[4,512]{1,0:T(4,128)S(1)} %bitcast.139, ...), kind=kOutput, calls=%fused_computation.15.clone.1 | convolution fusion | flops 140902400 | bytes 5799937 | tf_op jit(solution)/shard_map/while/body/eval_jaxpr/hqk,khd->hqd/dot_general | solution.py:87
  164.0 1.0 constant_dynamic-slice_fusion.4
  165.2 3.1 %fusion.76 = (f32[4,512]{1,0:T(4,128)S(1)}, f32[4,512,512]{2,1,0:T(8,128)}) fusion(f32[4,512]{1,0:T(4,128)S(1)} %dynamic-slice_bitcast_fusion.2, f32[4,512]{1,0:T(4,128)S(1)} %bitcast.137, pred[512,512]{0,1:T(8,128)(4,1)S(1)} %broadcast_compare_fusion.2, bf16[512,4,64]{0,2,1:T(8,128)(2,1)S(1)} %bitcast.131, ...), kind=kOutput, calls=%fused_computation.7.clone.1 | convolution fusion | flops 139458560 | bytes 5005312 | tf_op jit(solution)/shard_map/while/body/eval_jaxpr/qhd,khd->hqk/dot_general | solution.py:77
  168.3 2.9 %fusion.77 = f32[4,512]{1,0:T(4,128)S(1)} fusion(f32[4,512,512]{2,1,0:T(8,128)} %get-tuple-element.330, f32[4,512]{1,0:T(4,128)S(1)} %select_maximum_fusion.2, f32[4,512]{1,0:T(4,128)S(1)} %dynamic-slice_bitcast_fusion.2, f32[4,512]{1,0:T(4,128)S(1)} %bitcast.138, pred[512,512]{0,1:T(8,128)(4,1)S(1)} %broadcast_compare_fusion.2), kind=kLoop, calls=%fused_computation.12.clone.1 | loop fusion | flops 6289408 | bytes 4489216 | tf_op jit(solution)/shard_map/while/body/eval_jaxpr/reduce_sum | solution.py:86
  171.2 1.0 constant_dynamic-slice_fusion.5
  172.3 3.5 %fusion.79 = f32[4,512,64]{1,2,0:T(8,128)S(1)} fusion(bf16[512,4,64]{0,2,1:T(8,128)(2,1)S(1)} %bitcast.132, f32[4,512,512]{2,1,0:T(8,128)} %get-tuple-element.330, f32[4,512]{1,0:T(4,128)S(1)} %select_maximum_fusion.2, f32[4,512]{1,0:T(4,128)S(1)} %dynamic-slice_bitcast_fusion.2, f32[4,512]{1,0:T(4,128)S(1)} %bitcast.139, ...), kind=kOutput, calls=%fused_computation.15.clone.1 | convolution fusion | flops 140902400 | bytes 5799937 | tf_op jit(solution)/shard_map/while/body/eval_jaxpr/hqk,khd->hqd/dot_general | solution.py:87
  175.9 1.0 constant_dynamic-slice_fusion.4
  177.1 3.1 %fusion.76 = (f32[4,512]{1,0:T(4,128)S(1)}, f32[4,512,512]{2,1,0:T(8,128)}) fusion(f32[4,512]{1,0:T(4,128)S(1)} %dynamic-slice_bitcast_fusion.2, f32[4,512]{1,0:T(4,128)S(1)} %bitcast.137, pred[512,512]{0,1:T(8,128)(4,1)S(1)} %broadcast_compare_fusion.2, bf16[512,4,64]{0,2,1:T(8,128)(2,1)S(1)} %bitcast.131, ...), kind=kOutput, calls=%fused_computation.7.clone.1 | convolution fusion | flops 139458560 | bytes 5005312 | tf_op jit(solution)/shard_map/while/body/eval_jaxpr/qhd,khd->hqk/dot_general | solution.py:77
  180.2 2.9 %fusion.77 = f32[4,512]{1,0:T(4,128)S(1)} fusion(f32[4,512,512]{2,1,0:T(8,128)} %get-tuple-element.330, f32[4,512]{1,0:T(4,128)S(1)} %select_maximum_fusion.2, f32[4,512]{1,0:T(4,128)S(1)} %dynamic-slice_bitcast_fusion.2, f32[4,512]{1,0:T(4,128)S(1)} %bitcast.138, pred[512,512]{0,1:T(8,128)(4,1)S(1)} %broadcast_compare_fusion.2), kind=kLoop, calls=%fused_computation.12.clone.1 | loop fusion | flops 6289408 | bytes 4489216 | tf_op jit(solution)/shard_map/while/body/eval_jaxpr/reduce_sum | solution.py:86
  183.2 1.0 constant_dynamic-slice_fusion.5
  184.3 3.5 %fusion.79 = f32[4,512,64]{1,2,0:T(8,128)S(1)} fusion(bf16[512,4,64]{0,2,1:T(8,128)(2,1)S(1)} %bitcast.132, f32[4,512,512]{2,1,0:T(8,128)} %get-tuple-element.330, f32[4,512]{1,0:T(4,128)S(1)} %select_maximum_fusion.2, f32[4,512]{1,0:T(4,128)S(1)} %dynamic-slice_bitcast_fusion.2, f32[4,512]{1,0:T(4,128)S(1)} %bitcast.139, ...), kind=kOutput, calls=%fused_computation.15.clone.1 | convolution fusion | flops 140902400 | bytes 5799937 | tf_op jit(solution)/shard_map/while/body/eval_jaxpr/hqk,khd->hqd/dot_general | solution.py:87
  187.8 1.0 constant_dynamic-slice_fusion.4
  189.0 3.1 %fusion.76 = (f32[4,512]{1,0:T(4,128)S(1)}, f32[4,512,512]{2,1,0:T(8,128)}) fusion(f32[4,512]{1,0:T(4,128)S(1)} %dynamic-slice_bitcast_fusion.2, f32[4,512]{1,0:T(4,128)S(1)} %bitcast.137, pred[512,512]{0,1:T(8,128)(4,1)S(1)} %broadcast_compare_fusion.2, bf16[512,4,64]{0,2,1:T(8,128)(2,1)S(1)} %bitcast.131, ...), kind=kOutput, calls=%fused_computation.7.clone.1 | convolution fusion | flops 139458560 | bytes 5005312 | tf_op jit(solution)/shard_map/while/body/eval_jaxpr/qhd,khd->hqk/dot_general | solution.py:77
  192.1 2.9 %fusion.77 = f32[4,512]{1,0:T(4,128)S(1)} fusion(f32[4,512,512]{2,1,0:T(8,128)} %get-tuple-element.330, f32[4,512]{1,0:T(4,128)S(1)} %select_maximum_fusion.2, f32[4,512]{1,0:T(4,128)S(1)} %dynamic-slice_bitcast_fusion.2, f32[4,512]{1,0:T(4,128)S(1)} %bitcast.138, pred[512,512]{0,1:T(8,128)(4,1)S(1)} %broadcast_compare_fusion.2), kind=kLoop, calls=%fused_computation.12.clone.1 | loop fusion | flops 6289408 | bytes 4489216 | tf_op jit(solution)/shard_map/while/body/eval_jaxpr/reduce_sum | solution.py:86
  195.1 1.0 constant_dynamic-slice_fusion.5
  196.2 3.5 %fusion.79 = f32[4,512,64]{1,2,0:T(8,128)S(1)} fusion(bf16[512,4,64]{0,2,1:T(8,128)(2,1)S(1)} %bitcast.132, f32[4,512,512]{2,1,0:T(8,128)} %get-tuple-element.330, f32[4,512]{1,0:T(4,128)S(1)} %select_maximum_fusion.2, f32[4,512]{1,0:T(4,128)S(1)} %dynamic-slice_bitcast_fusion.2, f32[4,512]{1,0:T(4,128)S(1)} %bitcast.139, ...), kind=kOutput, calls=%fused_computation.15.clone.1 | convolution fusion | flops 140902400 | bytes 5799937 | tf_op jit(solution)/shard_map/while/body/eval_jaxpr/hqk,khd->hqd/dot_general | solution.py:87
  199.8 1.0 constant_dynamic-slice_fusion.4
  201.0 3.1 %fusion.76 = (f32[4,512]{1,0:T(4,128)S(1)}, f32[4,512,512]{2,1,0:T(8,128)}) fusion(f32[4,512]{1,0:T(4,128)S(1)} %dynamic-slice_bitcast_fusion.2, f32[4,512]{1,0:T(4,128)S(1)} %bitcast.137, pred[512,512]{0,1:T(8,128)(4,1)S(1)} %broadcast_compare_fusion.2, bf16[512,4,64]{0,2,1:T(8,128)(2,1)S(1)} %bitcast.131, ...), kind=kOutput, calls=%fused_computation.7.clone.1 | convolution fusion | flops 139458560 | bytes 5005312 | tf_op jit(solution)/shard_map/while/body/eval_jaxpr/qhd,khd->hqk/dot_general | solution.py:77
  204.1 2.9 %fusion.77 = f32[4,512]{1,0:T(4,128)S(1)} fusion(f32[4,512,512]{2,1,0:T(8,128)} %get-tuple-element.330, f32[4,512]{1,0:T(4,128)S(1)} %select_maximum_fusion.2, f32[4,512]{1,0:T(4,128)S(1)} %dynamic-slice_bitcast_fusion.2, f32[4,512]{1,0:T(4,128)S(1)} %bitcast.138, pred[512,512]{0,1:T(8,128)(4,1)S(1)} %broadcast_compare_fusion.2), kind=kLoop, calls=%fused_computation.12.clone.1 | loop fusion | flops 6289408 | bytes 4489216 | tf_op jit(solution)/shard_map/while/body/eval_jaxpr/reduce_sum | solution.py:86
  207.0 1.0 constant_dynamic-slice_fusion.5
  208.1 3.5 %fusion.79 = f32[4,512,64]{1,2,0:T(8,128)S(1)} fusion(bf16[512,4,64]{0,2,1:T(8,128)(2,1)S(1)} %bitcast.132, f32[4,512,512]{2,1,0:T(8,128)} %get-tuple-element.330, f32[4,512]{1,0:T(4,128)S(1)} %select_maximum_fusion.2, f32[4,512]{1,0:T(4,128)S(1)} %dynamic-slice_bitcast_fusion.2, f32[4,512]{1,0:T(4,128)S(1)} %bitcast.139, ...), kind=kOutput, calls=%fused_computation.15.clone.1 | convolution fusion | flops 140902400 | bytes 5799937 | tf_op jit(solution)/shard_map/while/body/eval_jaxpr/hqk,khd->hqd/dot_general | solution.py:87
  211.7 1.0 constant_dynamic-slice_fusion.4
  212.9 3.1 %fusion.76 = (f32[4,512]{1,0:T(4,128)S(1)}, f32[4,512,512]{2,1,0:T(8,128)}) fusion(f32[4,512]{1,0:T(4,128)S(1)} %dynamic-slice_bitcast_fusion.2, f32[4,512]{1,0:T(4,128)S(1)} %bitcast.137, pred[512,512]{0,1:T(8,128)(4,1)S(1)} %broadcast_compare_fusion.2, bf16[512,4,64]{0,2,1:T(8,128)(2,1)S(1)} %bitcast.131, ...), kind=kOutput, calls=%fused_computation.7.clone.1 | convolution fusion | flops 139458560 | bytes 5005312 | tf_op jit(solution)/shard_map/while/body/eval_jaxpr/qhd,khd->hqk/dot_general | solution.py:77
  216.0 2.9 %fusion.77 = f32[4,512]{1,0:T(4,128)S(1)} fusion(f32[4,512,512]{2,1,0:T(8,128)} %get-tuple-element.330, f32[4,512]{1,0:T(4,128)S(1)} %select_maximum_fusion.2, f32[4,512]{1,0:T(4,128)S(1)} %dynamic-slice_bitcast_fusion.2, f32[4,512]{1,0:T(4,128)S(1)} %bitcast.138, pred[512,512]{0,1:T(8,128)(4,1)S(1)} %broadcast_compare_fusion.2), kind=kLoop, calls=%fused_computation.12.clone.1 | loop fusion | flops 6289408 | bytes 4489216 | tf_op jit(solution)/shard_map/while/body/eval_jaxpr/reduce_sum | solution.py:86
  218.9 1.0 constant_dynamic-slice_fusion.5
  220.1 3.5 %fusion.79 = f32[4,512,64]{1,2,0:T(8,128)S(1)} fusion(bf16[512,4,64]{0,2,1:T(8,128)(2,1)S(1)} %bitcast.132, f32[4,512,512]{2,1,0:T(8,128)} %get-tuple-element.330, f32[4,512]{1,0:T(4,128)S(1)} %select_maximum_fusion.2, f32[4,512]{1,0:T(4,128)S(1)} %dynamic-slice_bitcast_fusion.2, f32[4,512]{1,0:T(4,128)S(1)} %bitcast.139, ...), kind=kOutput, calls=%fused_computation.15.clone.1 | convolution fusion | flops 140902400 | bytes 5799937 | tf_op jit(solution)/shard_map/while/body/eval_jaxpr/hqk,khd->hqd/dot_general | solution.py:87
  223.7 0.8 fusion.33
  224.6 3.5 %all-to-all-start.1 = ((bf16[8,48,512]{2,1,0:T(8,128)(2,1)}), bf16[8,48,512]{2,1,0:T(8,128)(2,1)S(1)}, u32[]{:S(2)}, u32[]{:S(2)}) async-start(bf16[8,48,512]{2,1,0:T(8,128)(2,1)} %bitcast.135), calls=%async_computation.2 | async-start | bytes 786432 | tf_op jit(solution)/shard_map/all_to_all | solution.py:149
  228.2 22.6 %all-gather.9.cloned.1.call-done = bf16[512,1024]{0,1:T(8,128)(2,1)} async-done(((bf16[512,256]{0,1:T(8,128)(2,1)}), bf16[512,1024]{0,1:T(8,128)(2,1)}) %all-gather.9.cloned.1.call-update) | async-done | bytes 1048592 | tf_op jit(solution)/shard_map/all_gather | solution.py:103
  250.8 3.1 %convolution_convert_fusion.1 = bf16[512,512]{1,0:T(8,128)(2,1)} fusion(bf16[512,1024]{0,1:T(8,128)(2,1)} %all-gather.9.cloned.1.call-done, bf16[1024,512]{1,0:T(8,128)(2,1)} %param.28), kind=kOutput, calls=%fused_computation.38 | convolution fusion | flops 537133056 | bytes 2621440 | tf_op jit(solution)/shard_map/dot_general | solution.py:102
  253.8 1.2 gather_fusion.1
  255.3 1.4 multiply_reduce_fusion
  (122 shorter events, 7.8 us)
Async XLA Ops:
  7.2 62.1 %copy-start = (bf16[1,256,2048]{2,1,0:T(8,128)(2,1)S(1)}, bf16[1,256,2048]{2,1,0:T(8,128)(2,1)}, u32[]{:S(2)}) copy-start(bf16[1,256,2048]{2,1,0:T(8,128)(2,1)} %param.35) | copy-start | bytes 3145732
  7.2 59.9 %all-gather.11.cloned.1.call-start = ((), (), s32[]{:S(2)}) async-start(), calls=%async_computation.6 | async-start | bytes 1966080 | tf_op jit(solution)/shard_map/all_gather | solution.py:132
  15.8 21.5 %copy-start.6 = (f32[64]{0:T(128)S(1)}, f32[64]{0:T(128)}, u32[]{:S(2)}) copy-start(f32[64]{0:T(128)} %param.25) | copy-start | bytes 772
  15.8 23.8 %copy-start.8 = (f32[2048]{0:T(1024)S(1)}, f32[2048]{0:T(1024)}, u32[]{:S(2)}) copy-start(f32[2048]{0:T(1024)} %param.20) | copy-start | bytes 24580
  37.2 60.6 %all-gather.5.cloned.1.call-start = ((), (), s32[]{:S(2)}) async-start(), calls=%async_computation.3 | async-start | bytes 2359296 | tf_op jit(solution)/shard_map/all_gather | solution.py:61
  37.4 6.0 %copy-start.1 = (bf16[512,2048]{1,0:T(8,128)(2,1)S(1)}, bf16[512,2048]{1,0:T(8,128)(2,1)}, u32[]{:S(2)}) copy-start(bf16[512,2048]{1,0:T(8,128)(2,1)} %param.19) | copy-start | bytes 6291460
  42.4 3.8 %copy-start.5 = (f32[256]{0:T(256)S(1)}, f32[256]{0:T(256)}, u32[]{:S(2)}) copy-start(f32[256]{0:T(256)} %param.27) | copy-start | bytes 3076
  42.4 3.8 %copy-start.3 = (f32[512,4]{0,1:T(4,128)S(1)}, f32[512,4]{0,1:T(4,128)}, u32[]{:S(2)}) copy-start(f32[512,4]{0,1:T(4,128)} %param.26) | copy-start | bytes 24580
  43.3 84.7 %all-gather.7.cloned.1.call-start = ((), (), s32[]{:S(2)}) async-start(), calls=%async_computation.4 | async-start | bytes 2359296 | tf_op jit(solution)/shard_map/all_gather | solution.py:62
  46.1 16.4 %copy-start.7 = (f32[64]{0:T(128)S(1)}, f32[64]{0:T(128)}, u32[]{:S(2)}) copy-start(f32[64]{0:T(128)} %param.24) | copy-start | bytes 772
  46.1 178.5 %reduce-scatter.2.cloned.1.call-start = ((), (), s32[]{:S(2)}) async-start(), calls=%async_computation.7 | async-start | bytes 1966080 | tf_op jit(solution)/shard_map/reduce_scatter | solution.py:145
  69.3 58.7 %copy-start.2 = (f32[4,512,64]{1,2,0:T(8,128)S(1)}, f32[4,512,64]{1,2,0:T(8,128)}, u32[]{:S(2)}) copy-start(f32[4,512,64]{1,2,0:T(8,128)} %custom-call.2) | copy-start | bytes 1572868
  74.1 176.6 %all-gather.9.cloned.1.call-start = ((), (), s32[]{:S(2)}) async-start(), calls=%async_computation.5 | async-start | bytes 1310720 | tf_op jit(solution)/shard_map/all_gather | solution.py:103
  128.0 100.0 %copy-start.4 = (f32[128,2]{0,1:T(2,128)S(1)}, f32[128,2]{0,1:T(2,128)}, u32[]{:S(2)}) copy-start(f32[128,2]{0,1:T(2,128)} %param.32) | copy-start | bytes 3076
  224.6 29.3 %all-to-all-start.1 = ((bf16[8,48,512]{2,1,0:T(8,128)(2,1)}), bf16[8,48,512]{2,1,0:T(8,128)(2,1)S(1)}, u32[]{:S(2)}, u32[]{:S(2)}) async-start(bf16[8,48,512]{2,1,0:T(8,128)(2,1)} %bitcast.135), calls=%async_computation.2 | async-start | bytes 786432 | tf_op jit(solution)/shard_map/all_to_all | solution.py:149
Sparse Core Ops, SparseCore 0:
  37.3 29.6 all-gather.10
  68.6 29.1 all-gather.4
  99.4 28.5 all-gather.6
  130.8 30.5 reduce-scatter.1
  224.6 26.0 all-gather.8
where the time goes:
time: 265 us; the launch traced here: 263 us
  waiting for transfers between devices  80.8 us (30%)
  matrix products  70.6 us (27%)
  other arithmetic  34.9 us (13%)
  blocking collectives  32.8 us (12%)
  local copies, waits for them, and re-layouts  25.7 us (10%)
  between operations  14.1 us (5%)
  starting transfers between devices  3.85 us (1%)
    all_gather x1, waiting for transfers between devices, body(): value_piece = lax.all_gather(value_rows, 'ep', axis=0, tiled=True)  30.2 us
    dot_general x8, matrix products, block_step(): jnp.einsum('hqk,khd->hqd', expo_scores.astype(jnp.bfloat16), value_block,...  28.1 us
    dot_general x8, matrix products, block_step(): jnp.einsum('qhd,khd->hqk', queries, key_block, preferred_element_type=jnp...  24.7 us
    all_gather x1, waiting for transfers between devices, body(): key_piece = lax.all_gather(key_rows, 'ep', axis=0, tiled=True)  23.4 us
    reduce_sum x8, other arithmetic, block_step(): running_sum = running_sum * rescale + jnp.sum(expo_scores, axis=2)  23.4 us
    all_gather x1, waiting for transfers between devices, body(): lax.all_gather(head_out, 'tp', axis=1, tiled=True)  22.6 us
    all_to_all x1, blocking collectives, body(): lax.all_to_all(share_part, 'ep', split_axis=0, concat_axis=0, tiled=True)  18.8 us
    all_gather x1, blocking collectives, body(): all_gates = lax.all_gather(log_cache, 'ep', axis=0, tiled=True)  14 us
  transfers between devices with their start and end apart: 6, of which 4 were waited for; matrix products, arithmetic and copies ran while one was open for 45% of the time, Pallas kernels for 0%

commit v1 on v0

--- a/solution.py
+++ b/solution.py
@@ -49,7 +49,6 @@
         .reshape(tok_rows, local_heads * HD)
     )
     value_rows = project(value_weight).astype(jnp.bfloat16).reshape(tok_rows, local_heads * HD)
-    all_gates = lax.all_gather(log_cache, "ep", axis=0, tiled=True)
     query_pos = lax.axis_index("ep") * tok_rows + jnp.arange(tok_rows, dtype=jnp.int32)
     query_gates = jnp.transpose(log_cache)[:, :, None]
     score_scale = HD ** (-0.5)
@@ -58,7 +57,14 @@
         jnp.zeros((local_heads, tok_rows), jnp.float32),
         jnp.zeros((local_heads, tok_rows, HD), jnp.float32),
     )
-    key_piece = lax.all_gather(key_rows, "ep", axis=0, tiled=True)
+
+    def clear_squares(local_x, x_in):
+        fresh = jnp.concatenate([local_x, x_in], axis=1)
+        extra = lax.all_gather(fresh, axis=0, axis_name="ep", tiled=True)
+        now = jnp.split(extra, [local_x.shape[1]], axis=1)
+        return now
+
+    all_gates, key_piece = clear_squares(log_cache, key_rows)
     value_piece = lax.all_gather(value_rows, "ep", axis=0, tiled=True)
     span_len = key_piece.shape[0]
     block_len = math.gcd(span_len, 512)

time: 265 us -> 280 us (1.057)
  waiting for transfers between devices: 80.8 us -> 106 us
  blocking collectives: 32.8 us -> 18.8 us
  local copies, waits for them, and re-layouts: 25.7 us -> 29.8 us
    all_gather x1, waiting for transfers between devices: 23.4 us -> 42.3 us  [clear_squares(): extra = lax.all_gather(fresh, axis=0, axis_name='ep', tiled=True)]
    all_gather x1, waiting for transfers between devices: 22.6 us -> 7.39 us  [body(): lax.all_gather(head_out, 'tp', axis=1, tiled=True)]
    all_gather x1 -> x0, blocking collectives: 14 us -> none  [body(): all_gates = lax.all_gather(log_cache, 'ep', axis=0, tiled=True)]
    all_gather x1, waiting for transfers between devices: 4.48 us -> 18.3 us  [body(): piece_now = lax.all_gather(arrived, 'tp', axis=2, tiled=True)]
    all_to_all x1, waiting for transfers between devices: 0.01 us -> 12.3 us  [body(): lax.all_to_all(summed.reshape(expert_count, capacity, out_cols), 'ep', sp...]
    all_gather x1, waiting for transfers between devices: 30.2 us -> 25.5 us  [body(): value_piece = lax.all_gather(value_rows, 'ep', axis=0, tiled=True)]
    split x0 -> x3, local copies, waits for them, and re-layouts: none -> 4.1 us  [clear_squares(): now = jnp.split(extra, [local_x.shape[1]], axis=1)]
  transfers between devices with their start and end apart: 6 -> 6, of which waited for: 4 -> 5; matrix products, arithmetic and copies ran while one was open for 45% -> 43% of each run, Pallas kernels for 0% -> 0%
where the time goes in v1:
time: 280 us; the launch traced here: 279 us
  waiting for transfers between devices  106 us (38%)
  matrix products  70.6 us (25%)
  other arithmetic  34.9 us (12%)
  local copies, waits for them, and re-layouts  29.8 us (11%)
  blocking collectives  18.8 us (7%)
  between operations  14.1 us (5%)
  starting transfers between devices  3.85 us (1%)
    all_gather x1, waiting for transfers between devices, clear_squares(): extra = lax.all_gather(fresh, axis=0, axis_name='ep', tiled=True)  42.3 us
    dot_general x8, matrix products, block_step(): jnp.einsum('hqk,khd->hqd', expo_scores.astype(jnp.bfloat16), value_block,...  28.1 us
    all_gather x1, waiting for transfers between devices, body(): value_piece = lax.all_gather(value_rows, 'ep', axis=0, tiled=True)  25.5 us
    dot_general x8, matrix products, block_step(): jnp.einsum('qhd,khd->hqk', queries, key_block, preferred_element_type=jnp...  24.7 us
    reduce_sum x8, other arithmetic, block_step(): running_sum = running_sum * rescale + jnp.sum(expo_scores, axis=2)  23.4 us
    all_to_all x1, blocking collectives, body(): lax.all_to_all(share_part, 'ep', split_axis=0, concat_axis=0, tiled=True)  18.8 us
    all_gather x1, waiting for transfers between devices, body(): piece_now = lax.all_gather(arrived, 'tp', axis=2, tiled=True)  18.3 us
    all_to_all x1, waiting for transfers between devices, body(): lax.all_to_all(summed.reshape(expert_count, capacity, out_cols), 'ep', sp...  12.3 us
  transfers between devices with their start and end apart: 6, of which 5 were waited for; matrix products, arithmetic and copies ran while one was open for 43% of the time, Pallas kernels for 0%

profile of v1, /device:TPU:0, one launch (start us, length us, event | category | flops | bytes accessed | tf_op | source)
XLA Modules:
  0.0 278.5 jit_solution(13499023942574114437)
XLA Ops:
  7.2 0.9 copy.25
  10.3 1.4 scatter_custom_fusion.1
  11.7 1.2 fusion.23
  13.0 1.5 scatter_custom_fusion
  14.5 1.2 fusion.25
  15.8 2.5 gather_fusion
  18.4 18.8 %all_to_all.10 = bf16[8,48,512]{2,1,0:T(8,128)(2,1)} all-to-all(bf16[8,48,512]{2,1,0:T(8,128)(2,1)S(1)} %dynamic-slice_select_fusion), channel_id=1, replica_groups=mesh['ep'=8,'tp'=4] {'ep'}, dimensions={0} | all-to-all | bytes 786432 | tf_op jit(solution)/shard_map/all_to_all | solution.py:137
  37.4 2.1 fusion.16
  39.5 2.9 %bitcast_reduce_fusion = (f32[512,4]{0,1:T(4,128)S(1)}, f32[512,256]{0,1:T(8,128)S(1)}) fusion(bf16[2048,256]{1,0:T(8,128)(2,1)} %param.22, bf16[512,2048]{1,0:T(8,128)(2,1)} %param.19, f32[2048]{0:T(1024)S(1)} %copy-done.8, f32[512]{0:T(512)S(1)} %add_rsqrt_fusion.3), kind=kOutput, calls=%fused_computation.60 | convolution fusion | flops 541325312 | bytes 3688448 | tf_op jit(solution)/shard_map/dot_general | solution.py:41
  43.5 2.7 convolution_convert_fusion.2
  46.4 2.2 multiply_reduce_fusion.1
  48.7 18.3 %all-gather.11.cloned.1.call-done = bf16[8,48,2048]{2,1,0:T(8,128)(2,1)} async-done(((bf16[8,48,512]{2,1,0:T(8,128)(2,1)}), bf16[8,48,2048]{2,1,0:T(8,128)(2,1)}) %all-gather.11.cloned.1.call-update) | async-done | bytes 1572880 | tf_op jit(solution)/shard_map/all_gather | solution.py:138
  67.0 2.3 convolution_bitcast_fusion.1
  69.3 4.7 %fusion.19 = bf16[8,1,48,2048]{3,2,0,1:T(8,128)(2,1)} fusion(bf16[1,256,2048]{2,1,0:T(8,128)(2,1)S(1)} %copy-done, bf16[8,48,2048]{2,1,0:T(8,128)(2,1)} %all-gather.11.cloned.1.call-done, bf16[1,2048,256]{2,1,0:T(8,128)(2,1)} %param.34, f32[8,1,48,256]{3,2,0,1:T(8,128)S(1)} %convolution_bitcast_fusion.1), kind=kOutput, calls=%fused_computation.35 | convolution fusion | flops 806682624 | bytes 5636096 | tf_op jit(solution)/shard_map/sjcf,jfd->sjcd/dot_general | solution.py:148
  74.3 42.3 %all-gather.5.cloned.1.call-done = f32[4096,260]{0,1:T(8,128)} async-done(((f32[512,260]{0,1:T(8,128)}), f32[4096,260]{0,1:T(8,128)}) %all-gather.5.cloned.1.call-update) | async-done | bytes 4259856 | tf_op jit(solution)/shard_map/all_gather | solution.py:63
  116.6 4.1 %split.8 = bf16[4096,256]{0,1:T(8,128)(2,1)} slice(f32[4096,260]{0,1:T(8,128)} %all-gather.5.cloned.1.call-done), slice={[0:4096], [4:260]} | slice | bytes 4194304 | tf_op jit(solution)/shard_map/split | solution.py:64
  120.7 25.5 %all-gather.7.cloned.1.call-done = bf16[4096,256]{1,0:T(8,128)(2,1)} async-done(((bf16[512,256]{1,0:T(8,128)(2,1)}), bf16[4096,256]{1,0:T(8,128)(2,1)}) %all-gather.7.cloned.1.call-update) | async-done | bytes 2097168 | tf_op jit(solution)/shard_map/all_gather | solution.py:68
  146.2 95.6 %while.18 = (s32[]{:T(128)}, f32[4,512]{1,0:T(4,128)S(1)}, f32[4,512]{1,0:T(4,128)S(1)}, f32[4,512,64]{1,2,0:T(8,128)S(1)}, bf16[4096,256]{0,1:T(8,128)(2,1)}, /...) while((s32[]{:T(128)}, f32[4,512]{1,0:T(4,128)S(1)}, ...), condition=%wide.region_6.7_spmd.clone, body=%wide.region_3.6_spmd.clone.sunk | while | flops 286927872 | bytes 17244372 | solution.py:101
  146.2 1.0 constant_dynamic-slice_fusion.4
  147.4 3.1 %fusion.77 = (f32[4,512]{1,0:T(4,128)S(1)}, f32[4,512,512]{2,1,0:T(8,128)}) fusion(f32[4,512]{1,0:T(4,128)S(1)} %dynamic-slice_bitcast_fusion.2, f32[4,512]{1,0:T(4,128)S(1)} %bitcast.139, pred[512,512]{0,1:T(8,128)(4,1)S(1)} %broadcast_compare_fusion.2, bf16[512,4,64]{0,2,1:T(8,128)(2,1)S(1)} %bitcast.133, ...), kind=kOutput, calls=%fused_computation.7.clone.1 | convolution fusion | flops 139458560 | bytes 5005312 | tf_op jit(solution)/shard_map/while/body/eval_jaxpr/qhd,khd->hqk/dot_general | solution.py:83
  150.5 2.9 %fusion.78 = f32[4,512]{1,0:T(4,128)S(1)} fusion(f32[4,512,512]{2,1,0:T(8,128)} %get-tuple-element.330, f32[4,512]{1,0:T(4,128)S(1)} %select_maximum_fusion.2, f32[4,512]{1,0:T(4,128)S(1)} %dynamic-slice_bitcast_fusion.2, f32[4,512]{1,0:T(4,128)S(1)} %bitcast.140, pred[512,512]{0,1:T(8,128)(4,1)S(1)} %broadcast_compare_fusion.2), kind=kLoop, calls=%fused_computation.12.clone.1 | loop fusion | flops 6289408 | bytes 4489216 | tf_op jit(solution)/shard_map/while/body/eval_jaxpr/reduce_sum | solution.py:92
  153.5 1.0 constant_dynamic-slice_fusion.5
  154.6 3.5 %fusion.80 = f32[4,512,64]{1,2,0:T(8,128)S(1)} fusion(bf16[512,4,64]{0,2,1:T(8,128)(2,1)S(1)} %bitcast.134, f32[4,512,512]{2,1,0:T(8,128)} %get-tuple-element.330, f32[4,512]{1,0:T(4,128)S(1)} %select_maximum_fusion.2, f32[4,512]{1,0:T(4,128)S(1)} %dynamic-slice_bitcast_fusion.2, f32[4,512]{1,0:T(4,128)S(1)} %bitcast.141, ...), kind=kOutput, calls=%fused_computation.15.clone.1 | convolution fusion | flops 140902400 | bytes 5799937 | tf_op jit(solution)/shard_map/while/body/eval_jaxpr/hqk,khd->hqd/dot_general | solution.py:93
  158.2 1.0 constant_dynamic-slice_fusion.4
  159.4 3.1 %fusion.77 = (f32[4,512]{1,0:T(4,128)S(1)}, f32[4,512,512]{2,1,0:T(8,128)}) fusion(f32[4,512]{1,0:T(4,128)S(1)} %dynamic-slice_bitcast_fusion.2, f32[4,512]{1,0:T(4,128)S(1)} %bitcast.139, pred[512,512]{0,1:T(8,128)(4,1)S(1)} %broadcast_compare_fusion.2, bf16[512,4,64]{0,2,1:T(8,128)(2,1)S(1)} %bitcast.133, ...), kind=kOutput, calls=%fused_computation.7.clone.1 | convolution fusion | flops 139458560 | bytes 5005312 | tf_op jit(solution)/shard_map/while/body/eval_jaxpr/qhd,khd->hqk/dot_general | solution.py:83
  162.5 3.0 %fusion.78 = f32[4,512]{1,0:T(4,128)S(1)} fusion(f32[4,512,512]{2,1,0:T(8,128)} %get-tuple-element.330, f32[4,512]{1,0:T(4,128)S(1)} %select_maximum_fusion.2, f32[4,512]{1,0:T(4,128)S(1)} %dynamic-slice_bitcast_fusion.2, f32[4,512]{1,0:T(4,128)S(1)} %bitcast.140, pred[512,512]{0,1:T(8,128)(4,1)S(1)} %broadcast_compare_fusion.2), kind=kLoop, calls=%fused_computation.12.clone.1 | loop fusion | flops 6289408 | bytes 4489216 | tf_op jit(solution)/shard_map/while/body/eval_jaxpr/reduce_sum | solution.py:92
  165.5 1.0 constant_dynamic-slice_fusion.5
  166.6 3.5 %fusion.80 = f32[4,512,64]{1,2,0:T(8,128)S(1)} fusion(bf16[512,4,64]{0,2,1:T(8,128)(2,1)S(1)} %bitcast.134, f32[4,512,512]{2,1,0:T(8,128)} %get-tuple-element.330, f32[4,512]{1,0:T(4,128)S(1)} %select_maximum_fusion.2, f32[4,512]{1,0:T(4,128)S(1)} %dynamic-slice_bitcast_fusion.2, f32[4,512]{1,0:T(4,128)S(1)} %bitcast.141, ...), kind=kOutput, calls=%fused_computation.15.clone.1 | convolution fusion | flops 140902400 | bytes 5799937 | tf_op jit(solution)/shard_map/while/body/eval_jaxpr/hqk,khd->hqd/dot_general | solution.py:93
  170.2 1.0 constant_dynamic-slice_fusion.4
  171.4 3.1 %fusion.77 = (f32[4,512]{1,0:T(4,128)S(1)}, f32[4,512,512]{2,1,0:T(8,128)}) fusion(f32[4,512]{1,0:T(4,128)S(1)} %dynamic-slice_bitcast_fusion.2, f32[4,512]{1,0:T(4,128)S(1)} %bitcast.139, pred[512,512]{0,1:T(8,128)(4,1)S(1)} %broadcast_compare_fusion.2, bf16[512,4,64]{0,2,1:T(8,128)(2,1)S(1)} %bitcast.133, ...), kind=kOutput, calls=%fused_computation.7.clone.1 | convolution fusion | flops 139458560 | bytes 5005312 | tf_op jit(solution)/shard_map/while/body/eval_jaxpr/qhd,khd->hqk/dot_general | solution.py:83
  174.5 2.9 %fusion.78 = f32[4,512]{1,0:T(4,128)S(1)} fusion(f32[4,512,512]{2,1,0:T(8,128)} %get-tuple-element.330, f32[4,512]{1,0:T(4,128)S(1)} %select_maximum_fusion.2, f32[4,512]{1,0:T(4,128)S(1)} %dynamic-slice_bitcast_fusion.2, f32[4,512]{1,0:T(4,128)S(1)} %bitcast.140, pred[512,512]{0,1:T(8,128)(4,1)S(1)} %broadcast_compare_fusion.2), kind=kLoop, calls=%fused_computation.12.clone.1 | loop fusion | flops 6289408 | bytes 4489216 | tf_op jit(solution)/shard_map/while/body/eval_jaxpr/reduce_sum | solution.py:92
  177.4 1.0 constant_dynamic-slice_fusion.5
  178.6 3.6 %fusion.80 = f32[4,512,64]{1,2,0:T(8,128)S(1)} fusion(bf16[512,4,64]{0,2,1:T(8,128)(2,1)S(1)} %bitcast.134, f32[4,512,512]{2,1,0:T(8,128)} %get-tuple-element.330, f32[4,512]{1,0:T(4,128)S(1)} %select_maximum_fusion.2, f32[4,512]{1,0:T(4,128)S(1)} %dynamic-slice_bitcast_fusion.2, f32[4,512]{1,0:T(4,128)S(1)} %bitcast.141, ...), kind=kOutput, calls=%fused_computation.15.clone.1 | convolution fusion | flops 140902400 | bytes 5799937 | tf_op jit(solution)/shard_map/while/body/eval_jaxpr/hqk,khd->hqd/dot_general | solution.py:93
  182.2 1.0 constant_dynamic-slice_fusion.4
  183.4 3.1 %fusion.77 = (f32[4,512]{1,0:T(4,128)S(1)}, f32[4,512,512]{2,1,0:T(8,128)}) fusion(f32[4,512]{1,0:T(4,128)S(1)} %dynamic-slice_bitcast_fusion.2, f32[4,512]{1,0:T(4,128)S(1)} %bitcast.139, pred[512,512]{0,1:T(8,128)(4,1)S(1)} %broadcast_compare_fusion.2, bf16[512,4,64]{0,2,1:T(8,128)(2,1)S(1)} %bitcast.133, ...), kind=kOutput, calls=%fused_computation.7.clone.1 | convolution fusion | flops 139458560 | bytes 5005312 | tf_op jit(solution)/shard_map/while/body/eval_jaxpr/qhd,khd->hqk/dot_general | solution.py:83
  186.5 2.9 %fusion.78 = f32[4,512]{1,0:T(4,128)S(1)} fusion(f32[4,512,512]{2,1,0:T(8,128)} %get-tuple-element.330, f32[4,512]{1,0:T(4,128)S(1)} %select_maximum_fusion.2, f32[4,512]{1,0:T(4,128)S(1)} %dynamic-slice_bitcast_fusion.2, f32[4,512]{1,0:T(4,128)S(1)} %bitcast.140, pred[512,512]{0,1:T(8,128)(4,1)S(1)} %broadcast_compare_fusion.2), kind=kLoop, calls=%fused_computation.12.clone.1 | loop fusion | flops 6289408 | bytes 4489216 | tf_op jit(solution)/shard_map/while/body/eval_jaxpr/reduce_sum | solution.py:92
  189.4 1.0 constant_dynamic-slice_fusion.5
  190.5 3.5 %fusion.80 = f32[4,512,64]{1,2,0:T(8,128)S(1)} fusion(bf16[512,4,64]{0,2,1:T(8,128)(2,1)S(1)} %bitcast.134, f32[4,512,512]{2,1,0:T(8,128)} %get-tuple-element.330, f32[4,512]{1,0:T(4,128)S(1)} %select_maximum_fusion.2, f32[4,512]{1,0:T(4,128)S(1)} %dynamic-slice_bitcast_fusion.2, f32[4,512]{1,0:T(4,128)S(1)} %bitcast.141, ...), kind=kOutput, calls=%fused_computation.15.clone.1 | convolution fusion | flops 140902400 | bytes 5799937 | tf_op jit(solution)/shard_map/while/body/eval_jaxpr/hqk,khd->hqd/dot_general | solution.py:93
  194.1 1.0 constant_dynamic-slice_fusion.4
  195.3 3.1 %fusion.77 = (f32[4,512]{1,0:T(4,128)S(1)}, f32[4,512,512]{2,1,0:T(8,128)}) fusion(f32[4,512]{1,0:T(4,128)S(1)} %dynamic-slice_bitcast_fusion.2, f32[4,512]{1,0:T(4,128)S(1)} %bitcast.139, pred[512,512]{0,1:T(8,128)(4,1)S(1)} %broadcast_compare_fusion.2, bf16[512,4,64]{0,2,1:T(8,128)(2,1)S(1)} %bitcast.133, ...), kind=kOutput, calls=%fused_computation.7.clone.1 | convolution fusion | flops 139458560 | bytes 5005312 | tf_op jit(solution)/shard_map/while/body/eval_jaxpr/qhd,khd->hqk/dot_general | solution.py:83
  198.4 2.9 %fusion.78 = f32[4,512]{1,0:T(4,128)S(1)} fusion(f32[4,512,512]{2,1,0:T(8,128)} %get-tuple-element.330, f32[4,512]{1,0:T(4,128)S(1)} %select_maximum_fusion.2, f32[4,512]{1,0:T(4,128)S(1)} %dynamic-slice_bitcast_fusion.2, f32[4,512]{1,0:T(4,128)S(1)} %bitcast.140, pred[512,512]{0,1:T(8,128)(4,1)S(1)} %broadcast_compare_fusion.2), kind=kLoop, calls=%fused_computation.12.clone.1 | loop fusion | flops 6289408 | bytes 4489216 | tf_op jit(solution)/shard_map/while/body/eval_jaxpr/reduce_sum | solution.py:92
  201.3 1.0 constant_dynamic-slice_fusion.5
  202.5 3.5 %fusion.80 = f32[4,512,64]{1,2,0:T(8,128)S(1)} fusion(bf16[512,4,64]{0,2,1:T(8,128)(2,1)S(1)} %bitcast.134, f32[4,512,512]{2,1,0:T(8,128)} %get-tuple-element.330, f32[4,512]{1,0:T(4,128)S(1)} %select_maximum_fusion.2, f32[4,512]{1,0:T(4,128)S(1)} %dynamic-slice_bitcast_fusion.2, f32[4,512]{1,0:T(4,128)S(1)} %bitcast.141, ...), kind=kOutput, calls=%fused_computation.15.clone.1 | convolution fusion | flops 140902400 | bytes 5799937 | tf_op jit(solution)/shard_map/while/body/eval_jaxpr/hqk,khd->hqd/dot_general | solution.py:93
  206.0 1.0 constant_dynamic-slice_fusion.4
  207.2 3.1 %fusion.77 = (f32[4,512]{1,0:T(4,128)S(1)}, f32[4,512,512]{2,1,0:T(8,128)}) fusion(f32[4,512]{1,0:T(4,128)S(1)} %dynamic-slice_bitcast_fusion.2, f32[4,512]{1,0:T(4,128)S(1)} %bitcast.139, pred[512,512]{0,1:T(8,128)(4,1)S(1)} %broadcast_compare_fusion.2, bf16[512,4,64]{0,2,1:T(8,128)(2,1)S(1)} %bitcast.133, ...), kind=kOutput, calls=%fused_computation.7.clone.1 | convolution fusion | flops 139458560 | bytes 5005312 | tf_op jit(solution)/shard_map/while/body/eval_jaxpr/qhd,khd->hqk/dot_general | solution.py:83
  210.3 2.9 %fusion.78 = f32[4,512]{1,0:T(4,128)S(1)} fusion(f32[4,512,512]{2,1,0:T(8,128)} %get-tuple-element.330, f32[4,512]{1,0:T(4,128)S(1)} %select_maximum_fusion.2, f32[4,512]{1,0:T(4,128)S(1)} %dynamic-slice_bitcast_fusion.2, f32[4,512]{1,0:T(4,128)S(1)} %bitcast.140, pred[512,512]{0,1:T(8,128)(4,1)S(1)} %broadcast_compare_fusion.2), kind=kLoop, calls=%fused_computation.12.clone.1 | loop fusion | flops 6289408 | bytes 4489216 | tf_op jit(solution)/shard_map/while/body/eval_jaxpr/reduce_sum | solution.py:92
  213.3 1.0 constant_dynamic-slice_fusion.5
  214.4 3.5 %fusion.80 = f32[4,512,64]{1,2,0:T(8,128)S(1)} fusion(bf16[512,4,64]{0,2,1:T(8,128)(2,1)S(1)} %bitcast.134, f32[4,512,512]{2,1,0:T(8,128)} %get-tuple-element.330, f32[4,512]{1,0:T(4,128)S(1)} %select_maximum_fusion.2, f32[4,512]{1,0:T(4,128)S(1)} %dynamic-slice_bitcast_fusion.2, f32[4,512]{1,0:T(4,128)S(1)} %bitcast.141, ...), kind=kOutput, calls=%fused_computation.15.clone.1 | convolution fusion | flops 140902400 | bytes 5799937 | tf_op jit(solution)/shard_map/while/body/eval_jaxpr/hqk,khd->hqd/dot_general | solution.py:93
  217.9 1.0 constant_dynamic-slice_fusion.4
  219.2 3.1 %fusion.77 = (f32[4,512]{1,0:T(4,128)S(1)}, f32[4,512,512]{2,1,0:T(8,128)}) fusion(f32[4,512]{1,0:T(4,128)S(1)} %dynamic-slice_bitcast_fusion.2, f32[4,512]{1,0:T(4,128)S(1)} %bitcast.139, pred[512,512]{0,1:T(8,128)(4,1)S(1)} %broadcast_compare_fusion.2, bf16[512,4,64]{0,2,1:T(8,128)(2,1)S(1)} %bitcast.133, ...), kind=kOutput, calls=%fused_computation.7.clone.1 | convolution fusion | flops 139458560 | bytes 5005312 | tf_op jit(solution)/shard_map/while/body/eval_jaxpr/qhd,khd->hqk/dot_general | solution.py:83
  222.3 2.9 %fusion.78 = f32[4,512]{1,0:T(4,128)S(1)} fusion(f32[4,512,512]{2,1,0:T(8,128)} %get-tuple-element.330, f32[4,512]{1,0:T(4,128)S(1)} %select_maximum_fusion.2, f32[4,512]{1,0:T(4,128)S(1)} %dynamic-slice_bitcast_fusion.2, f32[4,512]{1,0:T(4,128)S(1)} %bitcast.140, pred[512,512]{0,1:T(8,128)(4,1)S(1)} %broadcast_compare_fusion.2), kind=kLoop, calls=%fused_computation.12.clone.1 | loop fusion | flops 6289408 | bytes 4489216 | tf_op jit(solution)/shard_map/while/body/eval_jaxpr/reduce_sum | solution.py:92
  225.2 1.0 constant_dynamic-slice_fusion.5
  226.3 3.5 %fusion.80 = f32[4,512,64]{1,2,0:T(8,128)S(1)} fusion(bf16[512,4,64]{0,2,1:T(8,128)(2,1)S(1)} %bitcast.134, f32[4,512,512]{2,1,0:T(8,128)} %get-tuple-element.330, f32[4,512]{1,0:T(4,128)S(1)} %select_maximum_fusion.2, f32[4,512]{1,0:T(4,128)S(1)} %dynamic-slice_bitcast_fusion.2, f32[4,512]{1,0:T(4,128)S(1)} %bitcast.141, ...), kind=kOutput, calls=%fused_computation.15.clone.1 | convolution fusion | flops 140902400 | bytes 5799937 | tf_op jit(solution)/shard_map/while/body/eval_jaxpr/hqk,khd->hqd/dot_general | solution.py:93
  229.9 1.0 constant_dynamic-slice_fusion.4
  231.1 3.1 %fusion.77 = (f32[4,512]{1,0:T(4,128)S(1)}, f32[4,512,512]{2,1,0:T(8,128)}) fusion(f32[4,512]{1,0:T(4,128)S(1)} %dynamic-slice_bitcast_fusion.2, f32[4,512]{1,0:T(4,128)S(1)} %bitcast.139, pred[512,512]{0,1:T(8,128)(4,1)S(1)} %broadcast_compare_fusion.2, bf16[512,4,64]{0,2,1:T(8,128)(2,1)S(1)} %bitcast.133, ...), kind=kOutput, calls=%fused_computation.7.clone.1 | convolution fusion | flops 139458560 | bytes 5005312 | tf_op jit(solution)/shard_map/while/body/eval_jaxpr/qhd,khd->hqk/dot_general | solution.py:83
  234.2 2.9 %fusion.78 = f32[4,512]{1,0:T(4,128)S(1)} fusion(f32[4,512,512]{2,1,0:T(8,128)} %get-tuple-element.330, f32[4,512]{1,0:T(4,128)S(1)} %select_maximum_fusion.2, f32[4,512]{1,0:T(4,128)S(1)} %dynamic-slice_bitcast_fusion.2, f32[4,512]{1,0:T(4,128)S(1)} %bitcast.140, pred[512,512]{0,1:T(8,128)(4,1)S(1)} %broadcast_compare_fusion.2), kind=kLoop, calls=%fused_computation.12.clone.1 | loop fusion | flops 6289408 | bytes 4489216 | tf_op jit(solution)/shard_map/while/body/eval_jaxpr/reduce_sum | solution.py:92
  237.1 1.0 constant_dynamic-slice_fusion.5
  238.3 3.5 %fusion.80 = f32[4,512,64]{1,2,0:T(8,128)S(1)} fusion(bf16[512,4,64]{0,2,1:T(8,128)(2,1)S(1)} %bitcast.134, f32[4,512,512]{2,1,0:T(8,128)} %get-tuple-element.330, f32[4,512]{1,0:T(4,128)S(1)} %select_maximum_fusion.2, f32[4,512]{1,0:T(4,128)S(1)} %dynamic-slice_bitcast_fusion.2, f32[4,512]{1,0:T(4,128)S(1)} %bitcast.141, ...), kind=kOutput, calls=%fused_computation.15.clone.1 | convolution fusion | flops 140902400 | bytes 5799937 | tf_op jit(solution)/shard_map/while/body/eval_jaxpr/hqk,khd->hqd/dot_general | solution.py:93
  242.8 3.5 %all-to-all-start.1 = ((bf16[8,48,512]{2,1,0:T(8,128)(2,1)}), bf16[8,48,512]{2,1,0:T(8,128)(2,1)S(1)}, u32[]{:S(2)}, u32[]{:S(2)}) async-start(bf16[8,48,512]{2,1,0:T(8,128)(2,1)} %bitcast.137), calls=%async_computation.2 | async-start | bytes 786432 | tf_op jit(solution)/shard_map/all_to_all | solution.py:155
  246.4 12.3 %all-to-all-done.1 = bf16[8,48,512]{2,1,0:T(8,128)(2,1)S(1)} async-done(((bf16[8,48,512]{2,1,0:T(8,128)(2,1)}), bf16[8,48,512]{2,1,0:T(8,128)(2,1)S(1)}, u32[]{:S(2)}, u32[]{:S(2)}) %all-to-all-start.1) | async-done | bytes 393248 | tf_op jit(solution)/shard_map/all_to_all | solution.py:155
  258.7 1.2 gather_fusion.1
  260.2 1.4 multiply_reduce_fusion
  261.5 7.4 %all-gather.9.cloned.1.call-done = bf16[512,1024]{0,1:T(8,128)(2,1)} async-done(((bf16[512,256]{0,1:T(8,128)(2,1)}), bf16[512,1024]{0,1:T(8,128)(2,1)}) %all-gather.9.cloned.1.call-update) | async-done | bytes 1048592 | tf_op jit(solution)/shard_map/all_gather | solution.py:109
  268.9 3.1 %convolution_convert_fusion.1 = bf16[512,512]{1,0:T(8,128)(2,1)} fusion(bf16[512,1024]{0,1:T(8,128)(2,1)} %all-gather.9.cloned.1.call-done, bf16[1024,512]{1,0:T(8,128)(2,1)} %param.28), kind=kOutput, calls=%fused_computation.38 | convolution fusion | flops 537133056 | bytes 2621440 | tf_op jit(solution)/shard_map/dot_general | solution.py:108
  (125 shorter events, 8.8 us)
Async XLA Ops:
  7.2 62.1 %copy-start = (bf16[1,256,2048]{2,1,0:T(8,128)(2,1)S(1)}, bf16[1,256,2048]{2,1,0:T(8,128)(2,1)}, u32[]{:S(2)}) copy-start(bf16[1,256,2048]{2,1,0:T(8,128)(2,1)} %param.35) | copy-start | bytes 3145732
  7.2 59.8 %all-gather.11.cloned.1.call-start = ((), (), s32[]{:S(2)}) async-start(), calls=%async_computation.6 | async-start | bytes 1966080 | tf_op jit(solution)/shard_map/all_gather | solution.py:138
  15.8 21.5 %copy-start.6 = (f32[64]{0:T(128)S(1)}, f32[64]{0:T(128)}, u32[]{:S(2)}) copy-start(f32[64]{0:T(128)} %param.25) | copy-start | bytes 772
  15.8 23.7 %copy-start.8 = (f32[2048]{0:T(1024)S(1)}, f32[2048]{0:T(1024)}, u32[]{:S(2)}) copy-start(f32[2048]{0:T(1024)} %param.20) | copy-start | bytes 24580
  37.2 79.4 %all-gather.5.cloned.1.call-start = ((), (), s32[]{:S(2)}) async-start(), calls=%async_computation.3 | async-start | bytes 4866048 | tf_op jit(solution)/shard_map/all_gather | solution.py:63
  37.4 5.2 %copy-start.3 = (f32[512,4]{0,1:T(4,128)S(1)}, f32[512,4]{0,1:T(4,128)}, u32[]{:S(2)}) copy-start(f32[512,4]{0,1:T(4,128)} %param.26) | copy-start | bytes 24580
  39.5 4.1 %copy-start.1 = (bf16[512,2048]{1,0:T(8,128)(2,1)S(1)}, bf16[512,2048]{1,0:T(8,128)(2,1)}, u32[]{:S(2)}) copy-start(bf16[512,2048]{1,0:T(8,128)(2,1)} %param.19) | copy-start | bytes 6291460
  42.5 3.9 %copy-start.5 = (f32[256]{0:T(256)S(1)}, f32[256]{0:T(256)}, u32[]{:S(2)}) copy-start(f32[256]{0:T(256)} %param.27) | copy-start | bytes 3076
  43.5 102.7 %all-gather.7.cloned.1.call-start = ((), (), s32[]{:S(2)}) async-start(), calls=%async_computation.4 | async-start | bytes 2359296 | tf_op jit(solution)/shard_map/all_gather | solution.py:68
  46.2 2.4 copy-start.7
  46.3 196.5 %reduce-scatter.2.cloned.1.call-start = ((), (), s32[]{:S(2)}) async-start(), calls=%async_computation.7 | async-start | bytes 1966080 | tf_op jit(solution)/shard_map/reduce_scatter | solution.py:151
  74.0 72.2 %copy-start.2 = (f32[4,512,64]{1,2,0:T(8,128)S(1)}, f32[4,512,64]{1,2,0:T(8,128)}, u32[]{:S(2)}) copy-start(f32[4,512,64]{1,2,0:T(8,128)} %custom-call.2) | copy-start | bytes 1572868
  74.0 194.9 %all-gather.9.cloned.1.call-start = ((), (), s32[]{:S(2)}) async-start(), calls=%async_computation.5 | async-start | bytes 1310720 | tf_op jit(solution)/shard_map/all_gather | solution.py:109
  116.6 29.6 %slice-start = ((f32[4096,260]{0,1:T(8,128)}), f32[4096,4]{0,1:T(4,128)S(1)}, s32[]{:S(2)}) async-start(f32[4096,260]{0,1:T(8,128)} %all-gather.5.cloned.1.call-done), calls=%async_computation.8 | async-start | bytes 131072 | tf_op jit(solution)/shard_map/split | solution.py:64
  146.2 100.0 %copy-start.4 = (f32[128,2]{0,1:T(2,128)S(1)}, f32[128,2]{0,1:T(2,128)}, u32[]{:S(2)}) copy-start(f32[128,2]{0,1:T(2,128)} %param.32) | copy-start | bytes 3076
  242.8 15.9 %all-to-all-start.1 = ((bf16[8,48,512]{2,1,0:T(8,128)(2,1)}), bf16[8,48,512]{2,1,0:T(8,128)(2,1)S(1)}, u32[]{:S(2)}, u32[]{:S(2)}) async-start(bf16[8,48,512]{2,1,0:T(8,128)(2,1)} %bitcast.137), calls=%async_computation.2 | async-start | bytes 786432 | tf_op jit(solution)/shard_map/all_to_all | solution.py:155
Sparse Core Ops, SparseCore 0:
  37.3 29.6 all-gather.10
  68.6 47.9 all-gather.4
  118.2 27.9 all-gather.6
  149.0 30.5 reduce-scatter.1
  242.8 26.0 all-gather.8
